TPU v7x, 32 devices: a whole 2x2x4 slice. The times are simulated.
32 devices in a mesh: sp: 8 (over z, x), tp: 4 (over y, core).
Axes of the slice: x: 2, y: 2, z: 4, core: 2. Of those that a mesh axis runs over, the one named last changes fastest.
Arguments:
- queries: bfloat16 [5120, 2048], P('sp', 'tp'), may hold values from -164 to 164
- keys: bfloat16 [5120, 512], P('sp', 'tp'), may hold values from -6 to 6
- values: bfloat16 [5120, 512], P('sp', 'tp'), may hold values from -6 to 6
- sink: float32 [32], P('tp'), may hold values from 4 to 8
- stream: bfloat16 [5120, 2048], P(('sp', 'tp')), may hold values from -6 to 6
- out_weight: bfloat16 [2048, 2048], P('tp'), may hold values from -0.5390625 to 0.5390625
- norm_gain: float32 [2048], replicated, may hold values from 0.1 to 1.9
- gate_weight: bfloat16 [2048, 5632], P('sp', 'tp'), may hold values from -0.125 to 0.125
- up_weight: bfloat16 [2048, 5632], P('sp', 'tp'), may hold values from -0.125 to 0.125
- down_weight: bfloat16 [5632, 2048], P('tp', 'sp'), may hold values from -0.23925781 to 0.23925781
Outputs:
- result: bfloat16 [5120, 2048], P(('sp', 'tp'))
All inputs are finite; a program needn't handle non-finite values.
Results may differ from a plain program's by a relative error of at most 0.019.
Values may be sent and summed in bfloat16 or wider, within the bound.
A program may use at most 128 MiB of HBM per device.

v0:
```python
import jax
import jax.numpy as jnp
from jax import lax
from jax.sharding import PartitionSpec as P

HEAD = 64
WINDOW = 128


def padded_2(cells, sides, width):
    for axis, dim in sides:
        count = lax.axis_size(axis)
        ends = count - 1
        head = lax.slice_in_dim(cells, 0, width, axis=dim)
        tail = lax.slice_in_dim(cells, cells.shape[dim] - width, cells.shape[dim], axis=dim)
        cells = jnp.concatenate(
            [
                lax.ppermute(tail, axis, [(i, (i + 1) % count) for i in range(ends)]),
                cells,
                lax.ppermute(head, axis, [((i + 1) % count, i) for i in range(ends)]),
            ],
            axis=dim,
        )
    return cells


def rotary(block, start):
    length = block.shape[0]
    middle = HEAD // 2
    inverse = 1.0 / 10000.0 ** (jnp.arange(0, HEAD, 2, dtype=jnp.float32) / HEAD)
    places = (start + jnp.arange(length, dtype=jnp.int32)).astype(jnp.float32)
    angles = places[:, None, None] * inverse[None, None, :]
    cosine_table = jnp.cos(angles)
    sine_table = jnp.sin(angles)
    pieces = block.astype(jnp.float32).reshape(length, -1, HEAD)
    leading = pieces[..., :middle]
    trailing = pieces[..., middle:]
    turned = jnp.concatenate(
        [
            leading * cosine_table - trailing * sine_table,
            trailing * cosine_table + leading * sine_table,
        ],
        -1,
    )
    return turned.reshape(length, -1).astype(jnp.bfloat16)


def window_attend(queries, keys, values, sink):
    rows_here = queries.shape[0]
    start = lax.axis_index("sp") * rows_here
    length = lax.axis_size("sp") * rows_here
    blocks = rows_here // WINDOW
    kv_width = keys.shape[1]
    kv_count = kv_width // HEAD
    head_count = queries.shape[1] // HEAD
    group = head_count // kv_count
    turned_q = rotary(queries, start)
    turned_k = rotary(keys, start)
    paired = jnp.concatenate([turned_k, values], 1)
    padded = padded_2(paired, (("sp", 0),), WINDOW)
    framed = padded.reshape(blocks + 2, WINDOW, 2 * kv_width)
    banded = jnp.concatenate([framed[:-2], framed[1:-1], framed[2:]], axis=1)
    key_band = banded[..., :kv_width].reshape(blocks, 3 * WINDOW, kv_count, HEAD)
    value_band = banded[..., kv_width:].reshape(blocks, 3 * WINDOW, kv_count, HEAD)
    query_blocks = turned_q.reshape(blocks, WINDOW, kv_count, group, HEAD)
    scores = jnp.einsum(
        "nqkgd,nskd->nkgqs", query_blocks, key_band, preferred_element_type=jnp.float32
    ) * HEAD ** (-0.5)
    query_place = (
        start + jnp.arange(blocks)[:, None, None] * WINDOW + jnp.arange(WINDOW)[None, :, None]
    )
    key_place = (
        start
        + jnp.arange(blocks)[:, None, None] * WINDOW
        - WINDOW
        + jnp.arange(3 * WINDOW)[None, None, :]
    )
    valid = (jnp.abs(key_place - query_place) <= WINDOW) & (key_place >= 0) & (key_place < length)
    scores = jnp.where(valid[:, None, None], scores, -jnp.inf)
    sink_grid = sink.reshape(kv_count, group)[None, :, :, None]
    top = jnp.maximum(jnp.max(scores, -1), sink_grid)
    raised = jnp.exp(scores - top[..., None])
    denom = jnp.sum(raised, -1) + jnp.exp(sink_grid - top)
    weights = (raised / denom[..., None]).astype(jnp.bfloat16)
    output = jnp.einsum(
        "nkgqs,nskd->nqkgd", weights, value_band, preferred_element_type=jnp.float32
    )
    return output.astype(jnp.bfloat16).reshape(rows_here, head_count * HEAD)


def collect_weights(gate_weight, up_weight, down_weight):
    return (
        lax.all_gather(gate_weight, "sp", axis=0, tiled=True),
        lax.all_gather(up_weight, "sp", axis=0, tiled=True),
        lax.all_gather(down_weight, "sp", axis=1, tiled=True),
    )


def local(
    queries, keys, values, sink, stream, out_weight, norm_gain, gate_weight, up_weight, down_weight
):
    attended = window_attend(queries, keys, values, sink)
    gathered = collect_weights(gate_weight, up_weight, down_weight)
    gate_whole, up_whole, down_whole = gathered
    rows = attended
    projected = lax.psum_scatter(
        jnp.dot(rows, out_weight, preferred_element_type=jnp.float32),
        "tp",
        scatter_dimension=0,
        tiled=True,
    )
    mixed = (stream.astype(jnp.float32) + projected).astype(jnp.bfloat16)
    mixed_wide = mixed.astype(jnp.float32)
    scale = lax.rsqrt(jnp.mean(mixed_wide * mixed_wide, -1, keepdims=True) + 1e-06)
    normed = (mixed_wide * scale * norm_gain).astype(jnp.bfloat16)
    piece = lax.all_gather(normed, "tp", axis=0, tiled=True)
    gate = jnp.dot(piece, gate_whole, preferred_element_type=jnp.float32)
    upward = jnp.dot(piece, up_whole, preferred_element_type=jnp.float32)
    hidden = (jax.nn.silu(gate) * upward).astype(jnp.bfloat16)
    rows = hidden
    lowered = lax.psum_scatter(
        jnp.dot(rows, down_whole, preferred_element_type=jnp.float32).astype(jnp.bfloat16),
        "tp",
        scatter_dimension=0,
        tiled=True,
    ).astype(jnp.float32)
    return (mixed_wide + 0.5 * lowered).astype(jnp.bfloat16)


def solution(mesh):
    placed = (
        P("sp", "tp"),
        P("sp", "tp"),
        P("sp", "tp"),
        P("tp"),
        P(("sp", "tp"), None),
        P("tp", None),
        P(),
        P("sp", "tp"),
        P("sp", "tp"),
        P("tp", "sp"),
    )
    return jax.shard_map(
        local, mesh=mesh, in_specs=placed, out_specs=P(("sp", "tp"), None), check_vma=False
    )
```

profile of v0, /device:TPU:0, one launch (start us, length us, event | category | flops | bytes accessed | tf_op | source)
XLA Modules:
  0.0 420.8 jit_solution(13338107045309871906)
XLA Ops:
  7.4 1.2 copy.24
  8.6 1.1 copy.25
  9.7 0.4 multiply_cosine_fusion
  10.2 0.7 fusion.17
  10.9 5.5 %collective-permute-start = (bf16[128,256]{0,1:T(8,128)(2,1)}, bf16[128,256]{0,1:T(8,128)(2,1)}, u32[]{:S(2)}, u32[]{:S(2)}) collective-permute-start(bf16[128,256]{0,1:T(8,128)(2,1)} %get-tuple-element.16), channel_id=1, source_target_pairs={{0,4},{4,8},{8,12},{12,16},{16,20},{20,24},{24,28},{1,5},{5,9},{9,... | collective-permute-start | bytes 196616 | tf_op jit(solution)/shard_map/ppermute | solution.py:18
  16.4 1.3 collective-permute-start.1
  17.7 0.1 fusion.20
  17.7 0.1 iota_add_fusion
  17.8 0.1 iota_add_fusion.1
  17.9 1.4 copy.31
  19.3 0.1 convert.19
  19.4 0.2 subtract_convert_fusion
  19.5 1.2 fusion.11
  20.7 0.9 pad_maximum_fusion.1
  21.6 1.8 convert_element_type.55
  23.4 1.3 max.17
  24.8 2.1 pad_maximum_fusion.5
  26.8 1.9 copy.26
  28.7 1.9 copy.27
  30.6 1.9 copy.28
  32.5 1.2 pad_maximum_fusion
  33.7 1.2 fusion.24
  34.9 2.0 copy.30
  36.9 2.3 fusion.1
  39.2 0.1 broadcast_maximum_fusion
  39.3 1.9 fusion
  41.2 1.1 copy-done.1
  42.3 0.1 exponential_add_fusion
  42.4 0.3 copy.29
  42.6 5.4 %fusion.9 = bf16[5,128,2,4,64]{1,4,3,2,0:T(8,128)(2,1)S(1)} fusion(bf16[5,384,2,64,1]{1,3,4,2,0:T(8,128)(2,1)S(1)} %bitcast.59, f32[5,2,384,128,4]{3,2,4,1,0:T(8,128)} %copy-done.1, f32[5,2,4,128]{3,2,1,0:T(4,128)S(1)} %exponential_add_fusion, f32[5,2,4,128]{3,2,1,0:T(4,128)S(1)} %broadcast_maximum_fusion, pred[5,128,384]{1,2,0:T(8,128)(4,1)S(1)} %fusion.11), kind=kOutput, calls=%fused_computation.18 | convolution fusion | flops 261816320 | bytes 9297920 | tf_op jit(solution)/shard_map/nkgqs,nskd->nqkgd/dot_general | solution.py:85
  48.1 0.5 copy.34
  48.5 4.0 fusion.12
  52.5 0.0 all-gather.7.cloned.1.call-start
  52.6 0.5 all-gather.7.cloned.1.call-update
  53.2 53.3 %reduce-scatter.3.cloned.1.call-done = f32[160,2048]{1,0:T(8,128)} async-done(((f32[640,2048]{1,0:T(8,128)}), f32[160,2048]{1,0:T(8,128)}) %reduce-scatter.3.cloned.1.call-update) | async-done | bytes 1310736 | tf_op jit(solution)/shard_map/reduce_scatter | solution.py:106
  106.4 1.6 fusion.5
  108.0 1.1 fusion.7
  109.2 0.5 all-gather.11.cloned.1.call-update
  109.8 0.7 all-gather.9.cloned.1.call-update
  110.4 0.2 reduce-scatter.5.cloned.1.call-start
  110.7 39.1 %all-gather.7.cloned.1.call-done = bf16[2048,1408]{1,0:T(8,128)(2,1)} async-done(((bf16[256,1408]{1,0:T(8,128)(2,1)}), bf16[2048,1408]{1,0:T(8,128)(2,1)}) %all-gather.7.cloned.1.call-update) | async-done | bytes 5767184 | tf_op jit(solution)/shard_map/all_gather | solution.py:93
  149.8 25.0 %all-gather.5.cloned.1.call-done = bf16[640,2048]{1,0:T(8,128)(2,1)} async-done(((bf16[160,2048]{1,0:T(8,128)(2,1)}), bf16[640,2048]{1,0:T(8,128)(2,1)}) %all-gather.5.cloned.1.call-update) | async-done | bytes 2621456 | tf_op jit(solution)/shard_map/all_gather | solution.py:116
  174.8 9.4 %fusion.25 = f32[640,1408]{1,0:T(8,128)} fusion(bf16[640,2048]{1,0:T(8,128)(2,1)} %all-gather.5.cloned.1.call-done, bf16[2048,1408]{1,0:T(8,128)(2,1)} %all-gather.7.cloned.1.call-done), kind=kOutput, calls=%fused_computation.62 | convolution fusion | flops 3690987520 | bytes 11993088 | tf_op jit(solution)/shard_map/dot_general | solution.py:117
  184.2 85.4 %all-gather.11.cloned.1.call-done = bf16[1408,2048]{1,0:T(8,128)(2,1)} async-done(((bf16[1408,256]{1,0:T(8,128)(2,1)}), bf16[1408,2048]{1,0:T(8,128)(2,1)}) %all-gather.11.cloned.1.call-update) | async-done | bytes 5767184 | tf_op jit(solution)/shard_map/all_gather | solution.py:95
  269.6 92.5 %all-gather.9.cloned.1.call-done = bf16[2048,1408]{1,0:T(8,128)(2,1)} async-done(((bf16[256,1408]{1,0:T(8,128)(2,1)}), bf16[2048,1408]{1,0:T(8,128)(2,1)}) %all-gather.9.cloned.1.call-update) | async-done | bytes 5767184 | tf_op jit(solution)/shard_map/all_gather | solution.py:94
  362.1 16.1 %convolution_convert_fusion = bf16[640,2048]{1,0:T(8,128)(2,1)} fusion(bf16[1408,2048]{1,0:T(8,128)(2,1)} %all-gather.11.cloned.1.call-done, bf16[640,2048]{1,0:T(8,128)(2,1)} %all-gather.5.cloned.1.call-done, bf16[2048,1408]{1,0:T(8,128)(2,1)} %all-gather.9.cloned.1.call-done, f32[640,1408]{1,0:T(8,128)} %fusion.25), kind=kOutput, calls=%fused_computation.8 | convolution fusion | flops 7388692480 | bytes 20381696 | tf_op jit(solution)/shard_map/dot_general | solution.py:122
  378.3 32.8 %reduce-scatter.5.cloned.1.call-done = bf16[160,2048]{1,0:T(8,128)(2,1)} async-done(((bf16[640,2048]{1,0:T(8,128)(2,1)}), bf16[160,2048]{1,0:T(8,128)(2,1)}) %reduce-scatter.5.cloned.1.call-update) | async-done | bytes 655376 | tf_op jit(solution)/shard_map/reduce_scatter | solution.py:121
  411.1 2.1 fusion.8
  (29 shorter events, 0.3 us)
Async XLA Ops:
  7.4 41.2 %copy-start = (bf16[512,2048]{1,0:T(8,128)(2,1)S(1)}, bf16[512,2048]{1,0:T(8,128)(2,1)}, u32[]{:S(2)}) copy-start(bf16[512,2048]{1,0:T(8,128)(2,1)} %param.15) | copy-start | bytes 6291460
  7.4 99.1 %reduce-scatter.3.cloned.1.call-start = ((), (), s32[]{:S(2)}) async-start(), calls=%async_computation.2 | async-start | bytes 6553600 | tf_op jit(solution)/shard_map/reduce_scatter | solution.py:106
  10.2 7.6 %copy-start.3 = (bf16[640,2,64]{0,2,1:T(8,128)(2,1)}, bf16[640,2,64]{0,2,1:T(8,128)(2,1)S(1)}, u32[]{:S(2)}) copy-start(bf16[640,2,64]{0,2,1:T(8,128)(2,1)S(1)} %pad_maximum_fusion.7) | copy-start | bytes 491524
  10.9 13.9 %collective-permute-start = (bf16[128,256]{0,1:T(8,128)(2,1)}, bf16[128,256]{0,1:T(8,128)(2,1)}, u32[]{:S(2)}, u32[]{:S(2)}) collective-permute-start(bf16[128,256]{0,1:T(8,128)(2,1)} %get-tuple-element.16), channel_id=1, source_target_pairs={{0,4},{4,8},{8,12},{12,16},{16,20},{20,24},{24,28},{1,5},{5,9},{9,... | collective-permute-start | bytes 196616 | tf_op jit(solution)/shard_map/ppermute | solution.py:18
  16.4 8.4 %collective-permute-start.1 = (bf16[128,256]{0,1:T(8,128)(2,1)}, bf16[128,256]{0,1:T(8,128)(2,1)}, u32[]{:S(2)}, u32[]{:S(2)}) collective-permute-start(bf16[128,256]{0,1:T(8,128)(2,1)} %get-tuple-element.17), channel_id=1, source_target_pairs={{4,0},{8,4},{12,8},{16,12},{20,16},{24,20},{28,24},{5,1},{9,5},{13... | collective-permute-start | bytes 196616 | tf_op jit(solution)/shard_map/ppermute | solution.py:20
  36.9 2.3 copy-start.6
  39.2 3.1 copy-start.1
  39.3 3.0 copy-start.2
  52.5 53.9 %copy-start.4 = (bf16[160,2048]{1,0:T(8,128)(2,1)S(1)}, bf16[160,2048]{1,0:T(8,128)(2,1)}, u32[]{:S(2)}) copy-start(bf16[160,2048]{1,0:T(8,128)(2,1)} %param.14) | copy-start | bytes 1966084
  52.5 55.5 %copy-start.5 = (f32[2048]{0:T(1024)S(1)}, f32[2048]{0:T(1024)}, u32[]{:S(2)}) copy-start(f32[2048]{0:T(1024)} %param.16) | copy-start | bytes 24580
  52.5 97.2 %all-gather.7.cloned.1.call-start = ((), (), s32[]{:S(2)}) async-start(), calls=%async_computation.4 | async-start | bytes 6488064 | tf_op jit(solution)/shard_map/all_gather | solution.py:93
  53.1 121.7 %all-gather.5.cloned.1.call-start = ((), (), s32[]{:S(2)}) async-start(), calls=%async_computation.3 | async-start | bytes 3276800 | tf_op jit(solution)/shard_map/all_gather | solution.py:116
  109.1 160.5 %all-gather.11.cloned.1.call-start = ((), (), s32[]{:S(2)}) async-start(), calls=%async_computation.6 | async-start | bytes 6488064 | tf_op jit(solution)/shard_map/all_gather | solution.py:95
  109.7 252.4 %all-gather.9.cloned.1.call-start = ((), (), s32[]{:S(2)}) async-start(), calls=%async_computation.5 | async-start | bytes 6488064 | tf_op jit(solution)/shard_map/all_gather | solution.py:94
  110.4 300.6 %reduce-scatter.5.cloned.1.call-start = ((), (), s32[]{:S(2)}) async-start(), calls=%async_computation.7 | async-start | bytes 3276800 | tf_op jit(solution)/shard_map/reduce_scatter | solution.py:121
Sparse Core Ops, SparseCore 0:
  52.7 53.7 reduce-scatter.2
  378.4 32.6 reduce-scatter.4
Sparse Core Ops, SparseCore 1:
  55.2 94.5 all-gather.6
  151.2 23.5 all-gather.4
  176.7 92.8 all-gather.10
  271.8 90.3 all-gather.8
where the time goes:
time: 421 us
  waiting for transfers between devices  330 us (78%)
  matrix products  37.2 us (9%)
  local copies, waits for them, and re-layouts  17.4 us (4%)
  between operations  15.2 us (4%)
  other arithmetic  13.9 us (3%)
  starting transfers between devices  7.16 us (2%)
    all_gather x1, waiting for transfers between devices, collect_weights(): lax.all_gather(up_weight, 'sp', axis=0, tiled=True)  92.5 us
    all_gather x1, waiting for transfers between devices, collect_weights(): lax.all_gather(down_weight, 'sp', axis=1, tiled=True)  85.4 us
    reduce_scatter x1, waiting for transfers between devices, local(): lax.psum_scatter(jnp.dot(rows, out_weight, preferred_element_type=jnp.flo...  53.3 us
    all_gather x1, waiting for transfers between devices, collect_weights(): lax.all_gather(gate_weight, 'sp', axis=0, tiled=True)  39.1 us
    reduce_scatter x1, waiting for transfers between devices, local(): lax.psum_scatter(jnp.dot(rows, down_whole, preferred_element_type=jnp.flo...  32.8 us
    all_gather x1, waiting for transfers between devices, local(): piece = lax.all_gather(normed, 'tp', axis=0, tiled=True)  25 us
    dot_general x1, matrix products, local(): jnp.dot(rows, down_whole, preferred_element_type=jnp.float32)  16.1 us
    dot_general x1, matrix products, local(): gate = jnp.dot(piece, gate_whole, preferred_element_type=jnp.float32)  9.43 us
  transfers between devices with their start and end apart: 8, of which 6 were waited for; matrix products, arithmetic and copies ran while one was open for 5% of the time, Pallas kernels for 0%

commit v1 on v0

--- a/solution.py
+++ b/solution.py
@@ -92,7 +92,7 @@
     return (
         lax.all_gather(gate_weight, "sp", axis=0, tiled=True),
         lax.all_gather(up_weight, "sp", axis=0, tiled=True),
-        lax.all_gather(down_weight, "sp", axis=1, tiled=True),
+        jnp.concatenate(lax.all_gather(down_weight, "sp"), axis=1),
     )
 
 

time: 421 us -> 421 us (level)
  waiting for transfers between devices: 330 us -> 321 us
  local copies, waits for them, and re-layouts: 17.4 us -> 25.7 us
    all_gather x1, waiting for transfers between devices: 85.4 us -> 39.7 us  [collect_weights(): lax.all_gather(down_weight, 'sp')]
    all_gather x1, waiting for transfers between devices: 39.1 us -> 84.1 us  [collect_weights(): lax.all_gather(gate_weight, 'sp', axis=0, tiled=True)]
    reshape x0 -> x1, local copies, waits for them, and re-layouts: none -> 8.24 us  [collect_weights(): jnp.concatenate(lax.all_gather(down_weight, 'sp'), axis=1)]
    all_gather x1, waiting for transfers between devices: 92.5 us -> 84.9 us  [collect_weights(): lax.all_gather(up_weight, 'sp', axis=0, tiled=True)]
  transfers between devices with their start and end apart: 8 -> 8, of which waited for: 6 -> 6; matrix products, arithmetic and copies ran while one was open for 5% -> 7% of each run, Pallas kernels for 0% -> 0%
where the time goes in v1:
time: 421 us; the launch traced here: 420 us
  waiting for transfers between devices  321 us (76%)
  matrix products  37.4 us (9%)
  local copies, waits for them, and re-layouts  25.7 us (6%)
  between operations  15.2 us (4%)
  other arithmetic  13.9 us (3%)
  starting transfers between devices  7.15 us (2%)
    all_gather x1, waiting for transfers between devices, collect_weights(): lax.all_gather(up_weight, 'sp', axis=0, tiled=True)  84.9 us
    all_gather x1, waiting for transfers between devices, collect_weights(): lax.all_gather(gate_weight, 'sp', axis=0, tiled=True)  84.1 us
    reduce_scatter x1, waiting for transfers between devices, local(): lax.psum_scatter(jnp.dot(rows, out_weight, preferred_element_type=jnp.flo...  52.7 us
    all_gather x1, waiting for transfers between devices, collect_weights(): lax.all_gather(down_weight, 'sp')  39.7 us
    reduce_scatter x1, waiting for transfers between devices, local(): lax.psum_scatter(jnp.dot(rows, down_whole, preferred_element_type=jnp.flo...  32.8 us
    all_gather x1, waiting for transfers between devices, local(): piece = lax.all_gather(normed, 'tp', axis=0, tiled=True)  25 us
    dot_general x1, matrix products, local(): jnp.dot(rows, down_whole, preferred_element_type=jnp.float32)  16.2 us
    dot_general x1, matrix products, local(): gate = jnp.dot(piece, gate_whole, preferred_element_type=jnp.float32)  9.5 us
  transfers between devices with their start and end apart: 8, of which 6 were waited for; matrix products, arithmetic and copies ran while one was open for 7% of the time, Pallas kernels for 0%

profile of v1, /device:TPU:0, one launch (start us, length us, event | category | flops | bytes accessed | tf_op | source)
XLA Modules:
  0.0 420.3 jit_solution(14168148018029706920)
XLA Ops:
  7.4 1.2 copy.24
  8.6 1.1 copy.25
  9.7 0.4 multiply_cosine_fusion
  10.2 0.7 fusion.17
  10.9 5.5 %collective-permute-start = (bf16[128,256]{0,1:T(8,128)(2,1)}, bf16[128,256]{0,1:T(8,128)(2,1)}, u32[]{:S(2)}, u32[]{:S(2)}) collective-permute-start(bf16[128,256]{0,1:T(8,128)(2,1)} %get-tuple-element.16), channel_id=1, source_target_pairs={{0,4},{4,8},{8,12},{12,16},{16,20},{20,24},{24,28},{1,5},{5,9},{9,... | collective-permute-start | bytes 196616 | tf_op jit(solution)/shard_map/ppermute | solution.py:18
  16.4 1.3 collective-permute-start.1
  17.7 0.1 fusion.20
  17.7 0.1 iota_add_fusion
  17.8 0.1 iota_add_fusion.1
  17.9 1.4 copy.31
  19.3 0.1 convert.19
  19.4 0.2 subtract_convert_fusion
  19.5 1.2 fusion.11
  20.7 0.9 pad_maximum_fusion.1
  21.6 1.8 convert_element_type.55
  23.4 1.3 max.17
  24.8 2.1 pad_maximum_fusion.5
  26.8 1.9 copy.26
  28.7 1.9 copy.27
  30.6 1.9 copy.28
  32.5 1.2 pad_maximum_fusion
  33.7 1.2 fusion.24
  34.9 2.0 copy.30
  36.9 2.3 fusion.1
  39.3 0.1 broadcast_maximum_fusion
  39.3 1.9 fusion
  41.2 1.0 copy-done.2
  42.3 0.1 exponential_add_fusion
  42.4 0.3 copy.29
  42.6 5.4 %fusion.9 = bf16[5,128,2,4,64]{1,4,3,2,0:T(8,128)(2,1)S(1)} fusion(bf16[5,384,2,64,1]{1,3,4,2,0:T(8,128)(2,1)S(1)} %bitcast.65, f32[5,2,384,128,4]{3,2,4,1,0:T(8,128)} %copy-done.2, f32[5,2,4,128]{3,2,1,0:T(4,128)S(1)} %exponential_add_fusion, f32[5,2,4,128]{3,2,1,0:T(4,128)S(1)} %broadcast_maximum_fusion, pred[5,128,384]{1,2,0:T(8,128)(4,1)S(1)} %fusion.11), kind=kOutput, calls=%fused_computation.18 | convolution fusion | flops 261816320 | bytes 9297920 | tf_op jit(solution)/shard_map/nkgqs,nskd->nqkgd/dot_general | solution.py:85
  48.1 0.5 copy.34
  48.6 3.9 fusion.12
  52.6 0.5 all-gather.12.cloned.1.call-update
  53.2 0.5 all-gather.8.cloned.1.call-update
  53.8 52.7 %reduce-scatter.3.cloned.1.call-done = f32[160,2048]{1,0:T(8,128)} async-done(((f32[640,2048]{1,0:T(8,128)}), f32[160,2048]{1,0:T(8,128)}) %reduce-scatter.3.cloned.1.call-update) | async-done | bytes 1310736 | tf_op jit(solution)/shard_map/reduce_scatter | solution.py:106
  106.5 1.6 fusion.5
  108.1 1.1 fusion.7
  109.2 0.7 all-gather.10.cloned.1.call-update
  109.9 0.2 reduce-scatter.5.cloned.1.call-start
  110.1 39.7 %all-gather.12.cloned.1.call-done = bf16[11264,256]{1,0:T(8,128)(2,1)} async-done(((bf16[1408,256]{1,0:T(8,128)(2,1)}), bf16[11264,256]{1,0:T(8,128)(2,1)}) %all-gather.12.cloned.1.call-update) | async-done | bytes 5767184 | tf_op jit(solution)/shard_map/all_gather | solution.py:95
  149.8 8.2 %copy.35 = bf16[1408,8,256]{0,2,1:T(8,128)(2,1)} copy(bf16[1408,8,256]{2,0,1:T(8,128)(2,1)} %bitcast.54) | data formatting | bytes 11534336 | tf_op jit(solution)/shard_map/reshape | solution.py:95
  158.0 84.1 %all-gather.8.cloned.1.call-done = bf16[2048,1408]{1,0:T(8,128)(2,1)} async-done(((bf16[256,1408]{1,0:T(8,128)(2,1)}), bf16[2048,1408]{1,0:T(8,128)(2,1)}) %all-gather.8.cloned.1.call-update) | async-done | bytes 5767184 | tf_op jit(solution)/shard_map/all_gather | solution.py:93
  242.1 25.0 %all-gather.6.cloned.1.call-done = bf16[640,2048]{1,0:T(8,128)(2,1)} async-done(((bf16[160,2048]{1,0:T(8,128)(2,1)}), bf16[640,2048]{1,0:T(8,128)(2,1)}) %all-gather.6.cloned.1.call-update) | async-done | bytes 2621456 | tf_op jit(solution)/shard_map/all_gather | solution.py:116
  267.1 9.5 %fusion.25 = f32[640,1408]{1,0:T(8,128)} fusion(bf16[640,2048]{1,0:T(8,128)(2,1)} %all-gather.6.cloned.1.call-done, bf16[2048,1408]{1,0:T(8,128)(2,1)} %all-gather.8.cloned.1.call-done), kind=kOutput, calls=%fused_computation.62 | convolution fusion | flops 3690987520 | bytes 11993088 | tf_op jit(solution)/shard_map/dot_general | solution.py:117
  276.6 84.9 %all-gather.10.cloned.1.call-done = bf16[2048,1408]{1,0:T(8,128)(2,1)} async-done(((bf16[256,1408]{1,0:T(8,128)(2,1)}), bf16[2048,1408]{1,0:T(8,128)(2,1)}) %all-gather.10.cloned.1.call-update) | async-done | bytes 5767184 | tf_op jit(solution)/shard_map/all_gather | solution.py:94
  361.5 16.2 %convolution_convert_fusion = bf16[640,2048]{1,0:T(8,128)(2,1)} fusion(bf16[1408,2048]{0,1:T(8,128)(2,1)} %bitcast.55, bf16[640,2048]{1,0:T(8,128)(2,1)} %all-gather.6.cloned.1.call-done, bf16[2048,1408]{1,0:T(8,128)(2,1)} %all-gather.10.cloned.1.call-done, f32[640,1408]{1,0:T(8,128)} %fusion.25), kind=kOutput, calls=%fused_computation.8 | convolution fusion | flops 7388692480 | bytes 20381696 | tf_op jit(solution)/shard_map/dot_general | solution.py:122
  377.7 32.8 %reduce-scatter.5.cloned.1.call-done = bf16[160,2048]{1,0:T(8,128)(2,1)} async-done(((bf16[640,2048]{1,0:T(8,128)(2,1)}), bf16[160,2048]{1,0:T(8,128)(2,1)}) %reduce-scatter.5.cloned.1.call-update) | async-done | bytes 655376 | tf_op jit(solution)/shard_map/reduce_scatter | solution.py:121
  410.5 2.1 fusion.8
  (32 shorter events, 0.4 us)
Async XLA Ops:
  7.4 41.2 %copy-start = (bf16[512,2048]{1,0:T(8,128)(2,1)S(1)}, bf16[512,2048]{1,0:T(8,128)(2,1)}, u32[]{:S(2)}) copy-start(bf16[512,2048]{1,0:T(8,128)(2,1)} %param.15) | copy-start | bytes 6291460
  7.4 99.1 %reduce-scatter.3.cloned.1.call-start = ((), (), s32[]{:S(2)}) async-start(), calls=%async_computation.2 | async-start | bytes 6553600 | tf_op jit(solution)/shard_map/reduce_scatter | solution.py:106
  10.2 7.6 %copy-start.4 = (bf16[640,2,64]{0,2,1:T(8,128)(2,1)}, bf16[640,2,64]{0,2,1:T(8,128)(2,1)S(1)}, u32[]{:S(2)}) copy-start(bf16[640,2,64]{0,2,1:T(8,128)(2,1)S(1)} %pad_maximum_fusion.7) | copy-start | bytes 491524
  10.9 13.9 %collective-permute-start = (bf16[128,256]{0,1:T(8,128)(2,1)}, bf16[128,256]{0,1:T(8,128)(2,1)}, u32[]{:S(2)}, u32[]{:S(2)}) collective-permute-start(bf16[128,256]{0,1:T(8,128)(2,1)} %get-tuple-element.16), channel_id=1, source_target_pairs={{0,4},{4,8},{8,12},{12,16},{16,20},{20,24},{24,28},{1,5},{5,9},{9,... | collective-permute-start | bytes 196616 | tf_op jit(solution)/shard_map/ppermute | solution.py:18
  16.4 8.4 %collective-permute-start.1 = (bf16[128,256]{0,1:T(8,128)(2,1)}, bf16[128,256]{0,1:T(8,128)(2,1)}, u32[]{:S(2)}, u32[]{:S(2)}) collective-permute-start(bf16[128,256]{0,1:T(8,128)(2,1)} %get-tuple-element.17), channel_id=1, source_target_pairs={{4,0},{8,4},{12,8},{16,12},{20,16},{24,20},{28,24},{5,1},{9,5},{13... | collective-permute-start | bytes 196616 | tf_op jit(solution)/shard_map/ppermute | solution.py:20
  36.9 2.3 copy-start.7
  39.2 3.1 copy-start.2
  39.3 3.0 copy-start.3
  52.5 54.0 %copy-start.5 = (bf16[160,2048]{1,0:T(8,128)(2,1)S(1)}, bf16[160,2048]{1,0:T(8,128)(2,1)}, u32[]{:S(2)}) copy-start(bf16[160,2048]{1,0:T(8,128)(2,1)} %param.14) | copy-start | bytes 1966084
  52.5 55.6 %copy-start.6 = (f32[2048]{0:T(1024)S(1)}, f32[2048]{0:T(1024)}, u32[]{:S(2)}) copy-start(f32[2048]{0:T(1024)} %param.16) | copy-start | bytes 24580
  52.5 97.2 %all-gather.12.cloned.1.call-start = ((), (), s32[]{:S(2)}) async-start(), calls=%async_computation.7 | async-start | bytes 6488064 | tf_op jit(solution)/shard_map/all_gather | solution.py:95
  53.1 189.0 %all-gather.8.cloned.1.call-start = ((), (), s32[]{:S(2)}) async-start(), calls=%async_computation.4 | async-start | bytes 6488064 | tf_op jit(solution)/shard_map/all_gather | solution.py:93
  53.7 213.4 %all-gather.6.cloned.1.call-start = ((), (), s32[]{:S(2)}) async-start(), calls=%async_computation.3 | async-start | bytes 3276800 | tf_op jit(solution)/shard_map/all_gather | solution.py:116
  109.2 252.3 %all-gather.10.cloned.1.call-start = ((), (), s32[]{:S(2)}) async-start(), calls=%async_computation.5 | async-start | bytes 6488064 | tf_op jit(solution)/shard_map/all_gather | solution.py:94
  109.9 300.6 %reduce-scatter.5.cloned.1.call-start = ((), (), s32[]{:S(2)}) async-start(), calls=%async_computation.6 | async-start | bytes 3276800 | tf_op jit(solution)/shard_map/reduce_scatter | solution.py:121
  361.5 51.2 %copy-start.1 = (bf16[512,2048]{1,0:T(8,128)(2,1)S(1)}, bf16[512,2048]{1,0:T(8,128)(2,1)}, u32[]{:S(2)}) copy-start(bf16[512,2048]{1,0:T(8,128)(2,1)} %param.15) | copy-start | bytes 6291460
Sparse Core Ops, SparseCore 0:
  52.7 53.7 reduce-scatter.2
  377.9 32.6 reduce-scatter.4
Sparse Core Ops, SparseCore 1:
  55.2 94.5 all-gather.11
  151.8 90.2 all-gather.7
  243.6 23.5 all-gather.5
  269.4 92.1 all-gather.9
